TPU v7x, 32 devices: a whole 2x2x4 slice. The times are simulated.
32 devices in a mesh: sp: 4 (over y, x), tp: 8 (over z, core).
Axes of the slice: x: 2, y: 2, z: 4, core: 2. Of those that a mesh axis runs over, the one named last changes fastest.
Arguments:
- tokens: bfloat16 [8192, 2048], P('sp', 'tp'), may hold values from -6 to 6
- norm_gain: float32 [2048], replicated, may hold values from 0.1 to 1.9
- w_key: bfloat16 [2048, 1024], P(None, 'tp'), may hold values from -0.125 to 0.125
- w_decay: bfloat16 [2048, 1024], P(None, 'tp'), may hold values from -0.125 to 0.125
- w_value: bfloat16 [2048, 512], replicated, may hold values from -0.125 to 0.125
- decay_bias: float32 [1024], P('tp'), may hold values from 0 to 8.5
- gate_drift: float32 [8192], P('sp'), may hold values from -1 to 1
- queries: bfloat16 [1024], P('tp'), may hold values from -6 to 6
- out_gain: float32 [4, 512], P(None, 'sp'), may hold values from 0.1 to 1.9
Outputs:
- state_cache: bfloat16 [1024, 512], P('tp', 'sp')
- first_read: float32 [4, 512], P(None, 'sp')
All inputs are finite; a program needn't handle non-finite values.
Results may differ from a plain program's by a relative error of at most 0.009.
Values may be sent and summed in bfloat16 or wider, within the bound.
A program may use at most 128 MiB of HBM per device.

v0:
```python
import jax
import jax.numpy as jnp
from jax import lax
from jax.sharding import PartitionSpec as P

QUERY_KEY_HEADS = 4
KEY_CHANNELS = 256
VALUE_CHANNELS = 512
EPS = 1e-06
GATE_NORM = 16.0


def body(tokens, norm_gain, w_key, w_decay, w_value, decay_bias, gate_drift, queries, out_gain):
    gathered = lax.all_gather(tokens, "tp", axis=1, tiled=True)
    rows_f32 = gathered.astype(jnp.float32)
    inverse_rms = lax.rsqrt(jnp.mean(rows_f32 * rows_f32, axis=1, keepdims=True) + EPS)
    normed = (rows_f32 * inverse_rms * norm_gain[None, :]).astype(jnp.bfloat16)
    key_proj = jnp.dot(normed, w_key, preferred_element_type=jnp.float32).astype(jnp.bfloat16)
    gate_pre = jnp.dot(normed, w_decay, preferred_element_type=jnp.float32).astype(jnp.bfloat16)
    value_proj = jnp.dot(normed, w_value, preferred_element_type=jnp.float32).astype(jnp.bfloat16)
    log_decay = (
        jax.nn.log_sigmoid(gate_pre.astype(jnp.float32) + decay_bias[None, :] + gate_drift[:, None])
        / GATE_NORM
    )
    suffix = lax.cumsum(log_decay, axis=0, reverse=True)
    weighted = (key_proj.astype(jnp.float32) * jnp.exp(suffix - log_decay)).astype(jnp.bfloat16)
    partial_value = lax.dot_general(
        weighted, value_proj, (((0,), (0,)), ((), ())), preferred_element_type=jnp.float32
    )
    total_decay = suffix[0]
    channels = partial_value.shape[0]
    span_count = lax.axis_size("sp")
    spread = jnp.broadcast_to(total_decay[None, :, None], (1, channels, span_count))
    blocks, totals = (
        lax.all_to_all(partial_value[None], "sp", split_axis=2, concat_axis=0, tiled=True),
        lax.all_to_all(spread, "sp", split_axis=2, concat_axis=0, tiled=True),
    )
    later_sum = lax.cumsum(totals, axis=0, reverse=True) - totals
    matrix_state = jnp.sum(jnp.exp(later_sum) * blocks, axis=0)
    state_cache = matrix_state.astype(jnp.bfloat16)
    channel_ids = lax.axis_index("tp") * channels + jnp.arange(channels, dtype=jnp.int32)
    owners = (channel_ids // KEY_CHANNELS)[:, None] == jnp.arange(QUERY_KEY_HEADS, dtype=jnp.int32)[
        None, :
    ]
    query_of_head = jnp.where(
        owners, queries.astype(jnp.float32)[:, None] * KEY_CHANNELS ** (-0.5), 0.0
    )
    part_read = lax.dot_general(
        query_of_head, matrix_state, (((0,), (0,)), ((), ())), precision=lax.Precision.HIGHEST
    )
    summed_read = lax.psum(part_read, "tp")
    squares = lax.psum(jnp.sum(summed_read * summed_read, axis=1), "sp")
    first_read = summed_read * lax.rsqrt(squares / VALUE_CHANNELS + EPS)[:, None] * out_gain
    return (state_cache, first_read)


def solution(mesh):
    return jax.shard_map(
        body,
        mesh=mesh,
        in_specs=(
            P("sp", "tp"),
            P(),
            P(None, "tp"),
            P(None, "tp"),
            P(),
            P("tp"),
            P("sp"),
            P("tp"),
            P(None, "sp"),
        ),
        out_specs=(P("tp", "sp"), P(None, "sp")),
        check_vma=False,
    )
```

profile of v0, /device:TPU:0, one launch (start us, length us, event | category | flops | bytes accessed | tf_op | source)
XLA Modules:
  0.0 171.0 jit_solution(2722808447826279931)
XLA Ops:
  7.2 0.0 copy-start
  7.2 0.0 all-gather.2.cloned.1.call-start
  7.3 0.7 all-gather.2.cloned.1.call-update
  8.0 0.7 convert_multiply_fusion.2
  8.7 86.2 %all-gather.2.cloned.1.call-done = bf16[2048,2048]{1,0:T(8,128)(2,1)} async-done(((bf16[2048,256]{1,0:T(8,128)(2,1)}), bf16[2048,2048]{1,0:T(8,128)(2,1)}) %all-gather.2.cloned.1.call-update) | async-done | bytes 8388624 | tf_op jit(solution)/shard_map/all_gather | solution.py:14
  94.9 5.2 %fusion = f32[2048]{0:T(1024)S(1)} fusion(bf16[2048,2048]{1,0:T(8,128)(2,1)} %all-gather.2.cloned.1.call-done), kind=kLoop, calls=%fused_computation.2 | loop fusion | flops 12580864 | bytes 8396800 | tf_op jit(solution)/shard_map/reduce_sum | solution.py:16
  100.1 0.5 copy-done.1
  100.6 4.7 %fusion.12 = (f32[128,2048]{0,1:T(8,128)S(1)}, f32[2048,128]{1,0:T(8,128)}) fusion(f32[2048]{0:T(1024)S(1)} %copy-done.4, f32[128]{0:T(128)S(1)} %copy-done.6, bf16[2048,128]{1,0:T(8,128)(2,1)S(1)} %copy-done.3, bf16[2048,2048]{1,0:T(8,128)(2,1)S(1)} %copy-done.1, f32[2048]{0:T(1024)S(1)} %copy-done.5, f32[2048]{0:T(1024)S(1)} %add_rsqrt_fusion), kind=kOutput, calls=%fused_computation.19 | convolution fusion | flops 1093926912 | bytes 11035136 | tf_op jit(solution)/shard_map/dot_general | solution.py:19
  105.4 2.6 %fusion.21 = f32[128,16,128]{0,1,2:T(8,128)S(1)} fusion(f32[128,16,128]{0,2,1:T(8,128)S(1)} %bitcast.44), kind=kOutput, calls=%fused_computation.30 | output fusion | flops 33292288 | bytes 2097152 | tf_op jit(solution)/shard_map/reduce-window
  108.0 0.1 broadcast_add_fusion
  108.1 0.3 copy.17
  108.4 0.6 broadcast_in_dim.19
  109.0 3.6 %all-to-all-start = ((f32[1,128,4]{1,0,2:T(1,128)}), f32[1,128,4]{1,0,2:T(1,128)S(1)}, u32[]{:S(2)}, u32[]{:S(2)}) async-start(f32[1,128,4]{1,0,2:T(1,128)} %broadcast_in_dim.19), calls=%async_computation | async-start | bytes 4096 | tf_op jit(solution)/shard_map/all_to_all | solution.py:36
  112.6 7.6 %fusion.9 = bf16[2048,128]{1,0:T(8,128)(2,1)} fusion(bf16[2048,128]{1,0:T(8,128)(2,1)} %param.11, f32[2048,128]{1,0:T(8,128)S(1)} %bitcast.43, f32[2048,128]{1,0:T(8,128)} %get-tuple-element.5, bf16[2048,2048]{1,0:T(8,128)(2,1)} %all-gather.2.cloned.1.call-done, f32[2048]{0:T(1024)S(1)} %copy-done.5, f32[2048]{0:T(1024)S(1)} %add_rsqrt_fusion), kind=kOutput, calls=%fused_computation.16 | convolution fusion | flops 1093926912 | bytes 11550720 | tf_op jit(solution)/shard_map/dot_general | solution.py:18
  120.2 10.2 %fusion.10 = f32[128,512]{0,1:T(8,128)} fusion(bf16[2048,128]{1,0:T(8,128)(2,1)} %fusion.9, bf16[2048,512]{1,0:T(8,128)(2,1)S(1)} %copy-done, bf16[2048,2048]{1,0:T(8,128)(2,1)} %all-gather.2.cloned.1.call-done, f32[2048]{0:T(1024)S(1)} %copy-done.5, f32[2048]{0:T(1024)S(1)} %add_rsqrt_fusion), kind=kOutput, calls=%fused_computation.17 | convolution fusion | flops 4581228544 | bytes 11288576 | tf_op jit(solution)/shard_map/dot_general | solution.py:27
  130.4 0.0 all-to-all-done
  130.5 4.2 %all-to-all-start.1 = ((f32[1,128,512]{1,0,2:T(1,128)}), f32[1,128,512]{1,0,2:T(1,128)S(1)}, u32[]{:S(2)}, u32[]{:S(2)}) async-start(f32[1,128,512]{1,0,2:T(1,128)} %bitcast.18), calls=%async_computation.1 | async-start | bytes 524288 | tf_op jit(solution)/shard_map/all_to_all | solution.py:35
  134.7 5.3 %all-to-all-done.1 = f32[1,128,512]{1,0,2:T(1,128)S(1)} async-done(((f32[1,128,512]{1,0,2:T(1,128)}), f32[1,128,512]{1,0,2:T(1,128)S(1)}, u32[]{:S(2)}, u32[]{:S(2)}) %all-to-all-start.1) | async-done | bytes 262176 | tf_op jit(solution)/shard_map/all_to_all | solution.py:35
  140.0 0.3 fusion.23
  140.3 13.6 %psum.14 = f32[4,128]{1,0:T(4,128)S(1)} all-reduce(f32[4,128]{1,0:T(4,128)S(1)} %fusion.23), channel_id=1, replica_groups=mesh['sp'=4,'tp'=8] {'tp'}, use_global_device_ids=true, to_apply=%region_5.6 | all-reduce | flops 512 | bytes 4096 | tf_op jit(solution)/shard_map/psum | solution.py:51
  153.9 0.1 multiply_reduce_fusion.1
  154.1 8.7 %psum.15 = f32[4]{0:T(128)S(1)} all-reduce(f32[4]{0:T(128)S(1)} %multiply_reduce_fusion.1), channel_id=1, replica_groups=mesh['sp'=4,'tp'=8] {'sp'}, use_global_device_ids=true, to_apply=%region_7.8 | all-reduce | flops 4 | bytes 32 | tf_op jit(solution)/shard_map/psum | solution.py:52
  162.8 0.7 copy.19
  163.5 0.6 multiply_multiply_fusion
  (23 shorter events, 0.2 us)
Async XLA Ops:
  7.2 113.1 %copy-start = (bf16[2048,512]{1,0:T(8,128)(2,1)S(1)}, bf16[2048,512]{1,0:T(8,128)(2,1)}, u32[]{:S(2)}) copy-start(bf16[2048,512]{1,0:T(8,128)(2,1)} %param.13) | copy-start | bytes 6291460
  7.2 92.9 %copy-start.5 = (f32[2048]{0:T(1024)S(1)}, f32[2048]{0:T(1024)}, u32[]{:S(2)}) copy-start(f32[2048]{0:T(1024)} %param.10) | copy-start | bytes 24580
  7.2 92.9 %copy-start.3 = (bf16[2048,128]{1,0:T(8,128)(2,1)S(1)}, bf16[2048,128]{1,0:T(8,128)(2,1)}, u32[]{:S(2)}) copy-start(bf16[2048,128]{1,0:T(8,128)(2,1)} %param.12) | copy-start | bytes 1572868
  7.2 92.9 %copy-start.6 = (f32[128]{0:T(128)S(1)}, f32[128]{0:T(128)}, u32[]{:S(2)}) copy-start(f32[128]{0:T(128)} %param.14) | copy-start | bytes 1540
  7.2 92.9 %copy-start.4 = (f32[2048]{0:T(1024)S(1)}, f32[2048]{0:T(1024)}, u32[]{:S(2)}) copy-start(f32[2048]{0:T(1024)} %param.15) | copy-start | bytes 24580
  7.2 87.6 %all-gather.2.cloned.1.call-start = ((), (), s32[]{:S(2)}) async-start(), calls=%async_computation.2 | async-start | bytes 9437184 | tf_op jit(solution)/shard_map/all_gather | solution.py:14
  94.9 5.8 %copy-start.1 = (bf16[2048,2048]{1,0:T(8,128)(2,1)S(1)}, bf16[2048,2048]{1,0:T(8,128)(2,1)}, u32[]{:S(2)}) copy-start(bf16[2048,2048]{1,0:T(8,128)(2,1)} %all-gather.2.cloned.1.call-done) | copy-start | bytes 25165828
  109.0 21.5 %all-to-all-start = ((f32[1,128,4]{1,0,2:T(1,128)}), f32[1,128,4]{1,0,2:T(1,128)S(1)}, u32[]{:S(2)}, u32[]{:S(2)}) async-start(f32[1,128,4]{1,0,2:T(1,128)} %broadcast_in_dim.19), calls=%async_computation | async-start | bytes 4096 | tf_op jit(solution)/shard_map/all_to_all | solution.py:36
  120.2 43.3 %copy-start.2 = (f32[4,128]{1,0:T(4,128)S(1)}, f32[4,128]{1,0:T(4,128)}, u32[]{:S(2)}) copy-start(f32[4,128]{1,0:T(4,128)} %param.17) | copy-start | bytes 6148
  130.5 9.6 %all-to-all-start.1 = ((f32[1,128,512]{1,0,2:T(1,128)}), f32[1,128,512]{1,0,2:T(1,128)S(1)}, u32[]{:S(2)}, u32[]{:S(2)}) async-start(f32[1,128,512]{1,0,2:T(1,128)} %bitcast.18), calls=%async_computation.1 | async-start | bytes 524288 | tf_op jit(solution)/shard_map/all_to_all | solution.py:35
Sparse Core Ops, SparseCore 0:
  9.6 85.1 all-gather.1
where the time goes:
time: 171 us
  waiting for transfers between devices  92.2 us (54%)
  matrix products  22.8 us (13%)
  blocking collectives  22.4 us (13%)
  between operations  14.2 us (8%)
  other arithmetic  9.45 us (6%)
  starting transfers between devices  7.88 us (5%)
  local copies, waits for them, and re-layouts  2.17 us (1%)
    all_gather x1, waiting for transfers between devices, body(): gathered = lax.all_gather(tokens, 'tp', axis=1, tiled=True)  86.2 us
    psum x1, blocking collectives, body(): summed_read = lax.psum(part_read, 'tp')  13.6 us
    dot_general x1, matrix products, body(): lax.dot_general(weighted, value_proj, (((0,), (0,)), ((), ())), preferred...  10.2 us
    psum x1, blocking collectives, body(): squares = lax.psum(jnp.sum(summed_read * summed_read, axis=1), 'sp')  8.74 us
    dot_general x1, matrix products, body(): jnp.dot(normed, w_key, preferred_element_type=jnp.float32)  7.58 us
    all_to_all x1, waiting for transfers between devices, body(): lax.all_to_all(partial_value[None], 'sp', split_axis=2, concat_axis=0, ti...  5.33 us
    reduce_sum x1, other arithmetic, body(): jnp.mean(rows_f32 * rows_f32, axis=1, keepdims=True) + EPS  5.23 us
    dot_general x1, matrix products, body(): jnp.dot(normed, w_decay, preferred_element_type=jnp.float32)  4.74 us
  transfers between devices with their start and end apart: 3, of which 2 were waited for; matrix products, arithmetic and copies ran while one was open for 11% of the time, Pallas kernels for 0%

commit v1 on v0

--- a/solution.py
+++ b/solution.py
@@ -11,7 +11,12 @@
 
 
 def body(tokens, norm_gain, w_key, w_decay, w_value, decay_bias, gate_drift, queries, out_gain):
-    gathered = lax.all_gather(tokens, "tp", axis=1, tiled=True)
+    ring = [tokens]
+    for hop in range(7):
+        ring.append(lax.ppermute(ring[-1], "tp", [(dev, (dev + 1) % 8) for dev in range(8)]))
+    gathered = jnp.roll(
+        jnp.concatenate(ring[::-1], axis=1), (lax.axis_index("tp") + 1) * ring[0].shape[1], axis=1
+    )
     rows_f32 = gathered.astype(jnp.float32)
     inverse_rms = lax.rsqrt(jnp.mean(rows_f32 * rows_f32, axis=1, keepdims=True) + EPS)
     normed = (rows_f32 * inverse_rms * norm_gain[None, :]).astype(jnp.bfloat16)

time: 171 us -> 201 us (1.18)
  waiting for transfers between devices: 92.2 us -> 118 us
  local copies, waits for them, and re-layouts: 2.17 us -> 21.2 us
  between operations: 14.2 us -> 0.99 us
  other arithmetic: 9.45 us -> 6.04 us
    ppermute x0 -> x7, waiting for transfers between devices: none -> 112 us  [body(): lax.ppermute(ring[-1], 'tp', [(dev, (dev + 1) % 8) for dev in range(8)])]
    all_gather x1 -> x0, waiting for transfers between devices: 86.2 us -> none  [body(): gathered = lax.all_gather(tokens, 'tp', axis=1, tiled=True)]
    unnamed x15 -> x52, local copies, waits for them, and re-layouts: 1.24 us -> 20.1 us
    reduce_sum x1, other arithmetic: 5.23 us -> 1.71 us  [body(): jnp.mean(rows_f32 * rows_f32, axis=1, keepdims=True) + EPS]
  transfers between devices with their start and end apart: 3 -> 9, of which waited for: 2 -> 8; matrix products, arithmetic and copies ran while one was open for 11% -> 9% of each run, Pallas kernels for 0% -> 0%
where the time goes in v1:
time: 201 us
  waiting for transfers between devices  118 us (59%)
  matrix products  23.2 us (12%)
  blocking collectives  22.4 us (11%)
  local copies, waits for them, and re-layouts  21.2 us (11%)
  starting transfers between devices  8.96 us (4%)
  other arithmetic  6.04 us (3%)
    ppermute x7, waiting for transfers between devices, body(): lax.ppermute(ring[-1], 'tp', [(dev, (dev + 1) % 8) for dev in range(8)])  112 us
    unnamed x52, local copies, waits for them, and re-layouts  20.1 us
    psum x1, blocking collectives, body(): summed_read = lax.psum(part_read, 'tp')  13.6 us
    dot_general x1, matrix products, body(): lax.dot_general(weighted, value_proj, (((0,), (0,)), ((), ())), preferred...  10.2 us
    psum x1, blocking collectives, body(): squares = lax.psum(jnp.sum(summed_read * summed_read, axis=1), 'sp')  8.74 us
    dot_general x1, matrix products, body(): jnp.dot(normed, w_key, preferred_element_type=jnp.float32)  7.58 us
    all_to_all x1, waiting for transfers between devices, body(): lax.all_to_all(partial_value[None], 'sp', split_axis=2, concat_axis=0, ti...  5.33 us
    dot_general x1, matrix products, body(): jnp.dot(normed, w_decay, preferred_element_type=jnp.float32)  5.15 us
  transfers between devices with their start and end apart: 9, of which 8 were waited for; matrix products, arithmetic and copies ran while one was open for 9% of the time, Pallas kernels for 0%

profile of v1, /device:TPU:0, one launch (start us, length us, event | category | flops | bytes accessed | tf_op | source)
XLA Modules:
  0.0 200.5 jit_solution(13018355482418046786)
XLA Ops:
  1.2 16.7 %collective-permute-done = bf16[2048,256]{1,0:T(8,128)(2,1)S(1)} collective-permute-done((bf16[2048,256]{1,0:T(8,128)(2,1)}, bf16[2048,256]{1,0:T(8,128)(2,1)S(1)}, u32[]{:S(2)}, u32[]{:S(2)}) %collective-permute-start) | collective-permute-done | bytes 1048608 | tf_op jit(solution)/shard_map/ppermute | solution.py:16
  18.9 16.0 %collective-permute-done.1 = bf16[2048,256]{1,0:T(8,128)(2,1)S(1)} collective-permute-done((bf16[2048,256]{1,0:T(8,128)(2,1)S(1)}, bf16[2048,256]{1,0:T(8,128)(2,1)S(1)}, u32[]{:S(2)}, u32[]{:S(2)}) %collective-permute-start.1) | collective-permute-done | bytes 1048608 | tf_op jit(solution)/shard_map/ppermute | solution.py:16
  36.0 16.0 %collective-permute-done.2 = bf16[2048,256]{1,0:T(8,128)(2,1)S(1)} collective-permute-done((bf16[2048,256]{1,0:T(8,128)(2,1)S(1)}, bf16[2048,256]{1,0:T(8,128)(2,1)S(1)}, u32[]{:S(2)}, u32[]{:S(2)}) %collective-permute-start.2) | collective-permute-done | bytes 1048608 | tf_op jit(solution)/shard_map/ppermute | solution.py:16
  53.0 16.0 %collective-permute-done.3 = bf16[2048,256]{1,0:T(8,128)(2,1)S(1)} collective-permute-done((bf16[2048,256]{1,0:T(8,128)(2,1)S(1)}, bf16[2048,256]{1,0:T(8,128)(2,1)S(1)}, u32[]{:S(2)}, u32[]{:S(2)}) %collective-permute-start.3) | collective-permute-done | bytes 1048608 | tf_op jit(solution)/shard_map/ppermute | solution.py:16
  70.0 16.0 %collective-permute-done.4 = bf16[2048,256]{1,0:T(8,128)(2,1)S(1)} collective-permute-done((bf16[2048,256]{1,0:T(8,128)(2,1)S(1)}, bf16[2048,256]{1,0:T(8,128)(2,1)S(1)}, u32[]{:S(2)}, u32[]{:S(2)}) %collective-permute-start.4) | collective-permute-done | bytes 1048608 | tf_op jit(solution)/shard_map/ppermute | solution.py:16
  87.0 16.1 %collective-permute-done.5 = bf16[2048,256]{1,0:T(8,128)(2,1)} collective-permute-done((bf16[2048,256]{1,0:T(8,128)(2,1)S(1)}, bf16[2048,256]{1,0:T(8,128)(2,1)}, u32[]{:S(2)}, u32[]{:S(2)}) %collective-permute-start.5) | collective-permute-done | bytes 1048608 | tf_op jit(solution)/shard_map/ppermute | solution.py:16
  104.0 15.5 %collective-permute-done.6 = bf16[2048,256]{1,0:T(8,128)(2,1)} collective-permute-done((bf16[2048,256]{1,0:T(8,128)(2,1)}, bf16[2048,256]{1,0:T(8,128)(2,1)}, u32[]{:S(2)}, u32[]{:S(2)}) %collective-permute-start.6) | collective-permute-done | bytes 1048608 | tf_op jit(solution)/shard_map/ppermute | solution.py:16
  120.8 1.4 constant_dynamic-update-slice_fusion.14
  122.2 1.4 constant_dynamic-update-slice_fusion.13
  123.6 1.4 constant_dynamic-update-slice_fusion.12
  125.0 1.4 constant_dynamic-update-slice_fusion.11
  126.4 1.4 constant_dynamic-update-slice_fusion.10
  127.8 1.4 constant_dynamic-update-slice_fusion.9
  131.9 1.4 constant_dynamic-update-slice_fusion.6
  134.2 1.7 fusion
  136.0 5.1 %fusion.12 = (f32[128,2048]{0,1:T(8,128)S(1)}, f32[2048,128]{1,0:T(8,128)}) fusion(f32[2048]{0:T(1024)S(1)} %copy-done.15, f32[128]{0:T(128)S(1)} %copy-done.17, bf16[2048,128]{1,0:T(8,128)(2,1)S(1)} %copy-done.14, f32[2048]{0:T(1024)S(1)} %copy-done.16, f32[2048]{0:T(1024)S(1)} %add_rsqrt_fusion, ...), kind=kOutput, calls=%fused_computation.19 | convolution fusion | flops 1093926912 | bytes 11035140 | tf_op jit(solution)/shard_map/dot_general | solution.py:24
  141.1 2.6 %fusion.21 = f32[128,16,128]{0,1,2:T(8,128)S(1)} fusion(f32[128,16,128]{0,2,1:T(8,128)S(1)} %bitcast.44), kind=kOutput, calls=%fused_computation.30 | output fusion | flops 33292288 | bytes 2097152 | tf_op jit(solution)/shard_map/reduce-window
  144.8 4.2 %all-to-all-start = ((f32[1,128,4]{1,0,2:T(1,128)}), f32[1,128,4]{1,0,2:T(1,128)S(1)}, u32[]{:S(2)}, u32[]{:S(2)}) async-start(f32[1,128,4]{1,0,2:T(1,128)} %broadcast_in_dim.19), calls=%async_computation | async-start | bytes 4096 | tf_op jit(solution)/shard_map/all_to_all | solution.py:41
  149.0 7.6 %fusion.9 = bf16[2048,128]{1,0:T(8,128)(2,1)} fusion(bf16[2048,128]{1,0:T(8,128)(2,1)} %param.11, f32[2048,128]{1,0:T(8,128)S(1)} %bitcast.43, f32[2048,128]{1,0:T(8,128)} %get-tuple-element.5, f32[2048]{0:T(1024)S(1)} %copy-done.16, f32[2048]{0:T(1024)S(1)} %add_rsqrt_fusion, bf16[2048,4096]{1,0:T(8,128)(2,1)} %copy-done.1, s32[]{:T(128)S(6)} %select_n.35), kind=kOutput, calls=%fused_computation.16 | convolution fusion | flops 1093926912 | bytes 11550724 | tf_op jit(solution)/shard_map/dot_general | solution.py:23
  156.6 10.2 %fusion.10 = f32[128,512]{0,1:T(8,128)} fusion(bf16[2048,128]{1,0:T(8,128)(2,1)} %fusion.9, bf16[2048,512]{1,0:T(8,128)(2,1)S(1)} %copy-done, f32[2048]{0:T(1024)S(1)} %copy-done.16, f32[2048]{0:T(1024)S(1)} %add_rsqrt_fusion, bf16[2048,4096]{1,0:T(8,128)(2,1)} %copy-done.1, s32[]{:T(128)S(6)} %select_n.35), kind=kOutput, calls=%fused_computation.17 | convolution fusion | flops 4581228544 | bytes 11288580 | tf_op jit(solution)/shard_map/dot_general | solution.py:32
  166.8 4.2 %all-to-all-start.1 = ((f32[1,128,512]{1,0,2:T(1,128)}), f32[1,128,512]{1,0,2:T(1,128)S(1)}, u32[]{:S(2)}, u32[]{:S(2)}) async-start(f32[1,128,512]{1,0,2:T(1,128)} %bitcast.18), calls=%async_computation.1 | async-start | bytes 524288 | tf_op jit(solution)/shard_map/all_to_all | solution.py:40
  171.0 5.3 %all-to-all-done.1 = f32[1,128,512]{1,0,2:T(1,128)S(1)} async-done(((f32[1,128,512]{1,0,2:T(1,128)}), f32[1,128,512]{1,0,2:T(1,128)S(1)}, u32[]{:S(2)}, u32[]{:S(2)}) %all-to-all-start.1) | async-done | bytes 262176 | tf_op jit(solution)/shard_map/all_to_all | solution.py:40
  176.7 13.6 %psum.14 = f32[4,128]{1,0:T(4,128)S(1)} all-reduce(f32[4,128]{1,0:T(4,128)S(1)} %fusion.23), channel_id=1, replica_groups=mesh['sp'=4,'tp'=8] {'tp'}, use_global_device_ids=true, to_apply=%region_5.6 | all-reduce | flops 512 | bytes 4096 | tf_op jit(solution)/shard_map/psum | solution.py:56
  190.4 8.7 %psum.15 = f32[4]{0:T(128)S(1)} all-reduce(f32[4]{0:T(128)S(1)} %multiply_reduce_fusion.1), channel_id=1, replica_groups=mesh['sp'=4,'tp'=8] {'sp'}, use_global_device_ids=true, to_apply=%region_7.8 | all-reduce | flops 4 | bytes 32 | tf_op jit(solution)/shard_map/psum | solution.py:57
  (72 shorter events, 14.2 us)
Async XLA Ops:
  0.6 155.9 %copy-start = (bf16[2048,512]{1,0:T(8,128)(2,1)S(1)}, bf16[2048,512]{1,0:T(8,128)(2,1)}, u32[]{:S(2)}) copy-start(bf16[2048,512]{1,0:T(8,128)(2,1)} %param.13) | copy-start | bytes 6291460
  0.6 133.4 %copy-start.2 = (bf16[2048,256]{1,0:T(8,128)(2,1)S(1)}, bf16[2048,256]{1,0:T(8,128)(2,1)}, u32[]{:S(2)}) copy-start(bf16[2048,256]{1,0:T(8,128)(2,1)} %param.9) | copy-start | bytes 3145732
  0.7 17.3 %collective-permute-start = (bf16[2048,256]{1,0:T(8,128)(2,1)}, bf16[2048,256]{1,0:T(8,128)(2,1)S(1)}, u32[]{:S(2)}, u32[]{:S(2)}) collective-permute-start(bf16[2048,256]{1,0:T(8,128)(2,1)} %param.9), channel_id=1, source_target_pairs={{0,1},{1,2},{2,3},{3,4},{4,5},{5,6},{6,7},{7,0},{8,9},{9,10},{10,1... | collective-permute-start | bytes 3145736 | tf_op jit(solution)/shard_map/ppermute | solution.py:16
  18.9 16.0 %collective-permute-start.1 = (bf16[2048,256]{1,0:T(8,128)(2,1)S(1)}, bf16[2048,256]{1,0:T(8,128)(2,1)S(1)}, u32[]{:S(2)}, u32[]{:S(2)}) collective-permute-start(bf16[2048,256]{1,0:T(8,128)(2,1)S(1)} %collective-permute-done), channel_id=1, source_target_pairs={{0,1},{1,2},{2,3},{3,4},{4,5},{5,6},{6,7},{7,0},{8,9},{9,10},{10,1... | collective-permute-start | bytes 3145736 | tf_op jit(solution)/shard_map/ppermute | solution.py:16
  34.9 1.0 copy-start.5
  36.0 16.0 %collective-permute-start.2 = (bf16[2048,256]{1,0:T(8,128)(2,1)S(1)}, bf16[2048,256]{1,0:T(8,128)(2,1)S(1)}, u32[]{:S(2)}, u32[]{:S(2)}) collective-permute-start(bf16[2048,256]{1,0:T(8,128)(2,1)S(1)} %collective-permute-done.1), channel_id=1, source_target_pairs={{0,1},{1,2},{2,3},{3,4},{4,5},{5,6},{6,7},{7,0},{8,9},{9,10},{10,1... | collective-permute-start | bytes 3145736 | tf_op jit(solution)/shard_map/ppermute | solution.py:16
  52.0 1.0 copy-start.7
  53.0 16.0 %collective-permute-start.3 = (bf16[2048,256]{1,0:T(8,128)(2,1)S(1)}, bf16[2048,256]{1,0:T(8,128)(2,1)S(1)}, u32[]{:S(2)}, u32[]{:S(2)}) collective-permute-start(bf16[2048,256]{1,0:T(8,128)(2,1)S(1)} %collective-permute-done.2), channel_id=1, source_target_pairs={{0,1},{1,2},{2,3},{3,4},{4,5},{5,6},{6,7},{7,0},{8,9},{9,10},{10,1... | collective-permute-start | bytes 3145736 | tf_op jit(solution)/shard_map/ppermute | solution.py:16
  70.0 16.0 %collective-permute-start.4 = (bf16[2048,256]{1,0:T(8,128)(2,1)S(1)}, bf16[2048,256]{1,0:T(8,128)(2,1)S(1)}, u32[]{:S(2)}, u32[]{:S(2)}) collective-permute-start(bf16[2048,256]{1,0:T(8,128)(2,1)S(1)} %collective-permute-done.3), channel_id=1, source_target_pairs={{0,1},{1,2},{2,3},{3,4},{4,5},{5,6},{6,7},{7,0},{8,9},{9,10},{10,1... | collective-permute-start | bytes 3145736 | tf_op jit(solution)/shard_map/ppermute | solution.py:16
  87.0 16.1 %collective-permute-start.5 = (bf16[2048,256]{1,0:T(8,128)(2,1)S(1)}, bf16[2048,256]{1,0:T(8,128)(2,1)}, u32[]{:S(2)}, u32[]{:S(2)}) collective-permute-start(bf16[2048,256]{1,0:T(8,128)(2,1)S(1)} %collective-permute-done.4), channel_id=1, source_target_pairs={{0,1},{1,2},{2,3},{3,4},{4,5},{5,6},{6,7},{7,0},{8,9},{9,10},{10,1... | collective-permute-start | bytes 3145736 | tf_op jit(solution)/shard_map/ppermute | solution.py:16
  103.1 16.3 %collective-permute-start.6 = (bf16[2048,256]{1,0:T(8,128)(2,1)}, bf16[2048,256]{1,0:T(8,128)(2,1)}, u32[]{:S(2)}, u32[]{:S(2)}) collective-permute-start(bf16[2048,256]{1,0:T(8,128)(2,1)} %collective-permute-done.5), channel_id=1, source_target_pairs={{0,1},{1,2},{2,3},{3,4},{4,5},{5,6},{6,7},{7,0},{8,9},{9,10},{10,1... | collective-permute-start | bytes 3145736 | tf_op jit(solution)/shard_map/ppermute | solution.py:16
  103.1 30.2 %copy-start.12 = (bf16[2048,256]{1,0:T(8,128)(2,1)S(1)}, bf16[2048,256]{1,0:T(8,128)(2,1)}, u32[]{:S(2)}) copy-start(bf16[2048,256]{1,0:T(8,128)(2,1)} %copy-done.11) | copy-start | bytes 3145732
  103.1 30.3 %copy-start.10 = (bf16[2048,256]{1,0:T(8,128)(2,1)S(1)}, bf16[2048,256]{1,0:T(8,128)(2,1)}, u32[]{:S(2)}) copy-start(bf16[2048,256]{1,0:T(8,128)(2,1)} %copy-done.9) | copy-start | bytes 3145732
  103.1 30.5 %copy-start.8 = (bf16[2048,256]{1,0:T(8,128)(2,1)S(1)}, bf16[2048,256]{1,0:T(8,128)(2,1)}, u32[]{:S(2)}) copy-start(bf16[2048,256]{1,0:T(8,128)(2,1)} %copy-done.7) | copy-start | bytes 3145732
  103.1 30.6 %copy-start.6 = (bf16[2048,256]{1,0:T(8,128)(2,1)S(1)}, bf16[2048,256]{1,0:T(8,128)(2,1)}, u32[]{:S(2)}) copy-start(bf16[2048,256]{1,0:T(8,128)(2,1)} %copy-done.5) | copy-start | bytes 3145732
  103.1 30.8 %copy-start.4 = (bf16[2048,256]{1,0:T(8,128)(2,1)S(1)}, bf16[2048,256]{1,0:T(8,128)(2,1)}, u32[]{:S(2)}) copy-start(bf16[2048,256]{1,0:T(8,128)(2,1)} %copy-done.3) | copy-start | bytes 3145732
  124.9 11.0 %copy-start.14 = (bf16[2048,128]{1,0:T(8,128)(2,1)S(1)}, bf16[2048,128]{1,0:T(8,128)(2,1)}, u32[]{:S(2)}) copy-start(bf16[2048,128]{1,0:T(8,128)(2,1)} %param.12) | copy-start | bytes 1572868
  125.0 11.0 %copy-start.15 = (f32[2048]{0:T(1024)S(1)}, f32[2048]{0:T(1024)}, u32[]{:S(2)}) copy-start(f32[2048]{0:T(1024)} %param.15) | copy-start | bytes 24580
  125.0 11.0 %copy-start.16 = (f32[2048]{0:T(1024)S(1)}, f32[2048]{0:T(1024)}, u32[]{:S(2)}) copy-start(f32[2048]{0:T(1024)} %param.10) | copy-start | bytes 24580
  125.0 11.0 %copy-start.17 = (f32[128]{0:T(128)S(1)}, f32[128]{0:T(128)}, u32[]{:S(2)}) copy-start(f32[128]{0:T(128)} %param.14) | copy-start | bytes 1540
  134.2 6.9 %copy-start.1 = (bf16[2048,4096]{1,0:T(8,128)(2,1)}, bf16[2048,4096]{1,0:T(8,128)(2,1)S(1)}, u32[]{:S(2)}) copy-start(bf16[2048,4096]{1,0:T(8,128)(2,1)S(1)} %constant_dynamic-update-slice_fusion) | copy-start | bytes 50331652
  144.8 22.0 %all-to-all-start = ((f32[1,128,4]{1,0,2:T(1,128)}), f32[1,128,4]{1,0,2:T(1,128)S(1)}, u32[]{:S(2)}, u32[]{:S(2)}) async-start(f32[1,128,4]{1,0,2:T(1,128)} %broadcast_in_dim.19), calls=%async_computation | async-start | bytes 4096 | tf_op jit(solution)/shard_map/all_to_all | solution.py:41
  156.6 43.3 %copy-start.13 = (f32[4,128]{1,0:T(4,128)S(1)}, f32[4,128]{1,0:T(4,128)}, u32[]{:S(2)}) copy-start(f32[4,128]{1,0:T(4,128)} %param.17) | copy-start | bytes 6148
  166.8 9.6 %all-to-all-start.1 = ((f32[1,128,512]{1,0,2:T(1,128)}), f32[1,128,512]{1,0,2:T(1,128)S(1)}, u32[]{:S(2)}, u32[]{:S(2)}) async-start(f32[1,128,512]{1,0,2:T(1,128)} %bitcast.18), calls=%async_computation.1 | async-start | bytes 524288 | tf_op jit(solution)/shard_map/all_to_all | solution.py:40
  (3 other events, 2.9 us)
